TPU v7x, 32 devices: a whole 2x2x4 slice. The times are simulated.
32 devices in a mesh: dp: 4 (over y, x), kv: 4 (over z), tp: 2 (over core).
Axes of the slice: x: 2, y: 2, z: 4, core: 2. Of those that a mesh axis runs over, the one named last changes fastest.
Arguments:
- tokens: bfloat16 [4, 3072, 2048], P('dp', 'kv'), may hold values from -60 to 60
- query_weight: bfloat16 [2048, 1024], P(None, 'tp'), may hold values from -0.125 to 0.125
- key_weight: bfloat16 [2048, 256], P(None, 'tp'), may hold values from -0.125 to 0.125
- value_weight: bfloat16 [2048, 256], P(None, 'tp'), may hold values from -0.125 to 0.125
- out_weight: bfloat16 [1024, 2048], P('tp'), may hold values from -3 to 3
- norm_gain: float32 [2048], P('tp'), may hold values from 0.1 to 1.9
- chosen_owner: int32 [4, 24, 4], P('dp'), may hold values from -1 to 3, as said below
- chosen_part: int32 [4, 24, 4], P('dp'), may hold values from 0 to 11, as said below
Outputs:
- attended: bfloat16 [4, 3072, 2048], P('dp', 'kv', 'tp')
Inputs may be any that keep to these rules, and one draw needn't show every extreme that they name: `chosen_owner`: within a row the indices other than -1 are different. Every named key block lies wholly before its query block's first position. Among the 6 rows of one index of kv, no index is named by more than 6 rows. `chosen_part`: 0 where the owner is -1.
All inputs are finite; a program needn't handle non-finite values.
Results may differ from a plain program's by a relative error of at most 0.014.
The roundings to bfloat16 on the way count: a program that leaves them out, or rounds other values in their place, can miss the bound.
Values may be sent and summed in bfloat16 or wider, within the bound.
A program may use at most 128 MiB of HBM per device.

v0:
```python
import jax
import jax.numpy as jnp
from jax import lax
from jax.sharding import PartitionSpec as P

D = 2048
HEAD_DIM = 64
QUERY_BLOCK = 128
KEY_BLOCK = 64


rope_base = 10000.0
norm_eps = 1e-06


def rotate(head_rows, positions):
    half_dim = head_rows.shape[-1] // 2
    frequency = rope_base ** (-jnp.arange(half_dim, dtype=jnp.float32) / half_dim)
    angles = positions.astype(jnp.float32)[:, None] * frequency
    cosine = jnp.cos(angles)[:, None, :]
    sine_part = jnp.sin(angles)[:, None, :]
    first_half = head_rows[..., :half_dim]
    second_half = head_rows[..., half_dim:]
    return jnp.concatenate(
        [
            first_half * cosine - second_half * sine_part,
            second_half * cosine + first_half * sine_part,
        ],
        axis=-1,
    )


def rank_within(flat_ids):
    entry_count = flat_ids.shape[0]
    same_owner = flat_ids[:, None] == flat_ids[None, :]
    earlier = jnp.arange(entry_count)[None, :] < jnp.arange(entry_count)[:, None]
    return jnp.sum(jnp.logical_and(same_owner, earlier), axis=1)


def body(
    tokens, query_weight, key_weight, value_weight, out_weight, norm_gain, chosen_owner, chosen_part
):
    row_data = tokens[0]
    tok_count = row_data.shape[0]
    devices = lax.axis_size("kv")
    my_index = lax.axis_index("kv")
    positions = my_index * tok_count + jnp.arange(tok_count, dtype=jnp.int32)
    heads_here = query_weight.shape[1] // HEAD_DIM
    kv_here = key_weight.shape[1] // HEAD_DIM
    group_size = heads_here // kv_here
    kv_width = kv_here * HEAD_DIM
    queries = rotate(
        jnp.dot(row_data, query_weight, preferred_element_type=jnp.float32).reshape(
            tok_count, heads_here, HEAD_DIM
        ),
        positions,
    ).astype(jnp.bfloat16)
    key_rows = (
        rotate(
            jnp.dot(row_data, key_weight, preferred_element_type=jnp.float32).reshape(
                tok_count, kv_here, HEAD_DIM
            ),
            positions,
        )
        .astype(jnp.bfloat16)
        .reshape(tok_count, kv_width)
    )
    value_rows = jnp.dot(row_data, value_weight, preferred_element_type=jnp.float32).astype(
        jnp.bfloat16
    )
    per_device = tok_count // KEY_BLOCK
    qblocks = tok_count // QUERY_BLOCK
    chosen_count = chosen_owner.shape[2]
    owner_ids = chosen_owner[0]
    part_ids = chosen_part[0]
    mine_owner = lax.dynamic_slice_in_dim(owner_ids, my_index * qblocks, qblocks, 0).reshape(
        qblocks * chosen_count
    )
    mine_valid = mine_owner >= 0
    key_blocks = key_rows.reshape(per_device, KEY_BLOCK, kv_width)
    value_blocks = value_rows.reshape(per_device, KEY_BLOCK, kv_width)
    every_owner = owner_ids.reshape(devices, qblocks * chosen_count)
    every_part = part_ids.reshape(devices, qblocks * chosen_count)
    every_rank = jax.vmap(rank_within)(every_owner)
    slot_ids = jnp.arange(qblocks, dtype=jnp.int32)
    picked_mask = jnp.logical_and(
        (every_owner == my_index)[:, None, :], every_rank[:, None, :] == slot_ids[None, :, None]
    )
    wanted = jnp.sum(jnp.where(picked_mask, every_part[:, None, :], 0), axis=2)
    send_keys = key_blocks[wanted]
    send_values = value_blocks[wanted]
    got_keys, got_values = (
        lax.all_to_all(send_keys, "kv", split_axis=0, concat_axis=0, tiled=True),
        lax.all_to_all(send_values, "kv", split_axis=0, concat_axis=0, tiled=True),
    )
    slot_index = jnp.where(mine_valid, mine_owner * qblocks + rank_within(mine_owner), 0)
    picked_keys = got_keys.reshape(devices * qblocks, KEY_BLOCK, kv_width)[slot_index]
    picked_values = got_values.reshape(devices * qblocks, KEY_BLOCK, kv_width)[slot_index]
    block_queries = queries.reshape(qblocks, QUERY_BLOCK, kv_here, group_size, HEAD_DIM)
    chosen_keys = picked_keys.reshape(qblocks, chosen_count * KEY_BLOCK, kv_here, HEAD_DIM)
    chosen_values = picked_values.reshape(qblocks, chosen_count * KEY_BLOCK, kv_here, HEAD_DIM)
    all_keys = jnp.concatenate(
        [chosen_keys, key_rows.reshape(qblocks, QUERY_BLOCK, kv_here, HEAD_DIM)], axis=1
    )
    all_values = jnp.concatenate(
        [chosen_values, value_rows.reshape(qblocks, QUERY_BLOCK, kv_here, HEAD_DIM)], axis=1
    )
    key_valid = jnp.broadcast_to(
        mine_valid.reshape(qblocks, chosen_count, 1), (qblocks, chosen_count, KEY_BLOCK)
    ).reshape(qblocks, chosen_count * KEY_BLOCK)
    far_mask = jnp.broadcast_to(
        key_valid[:, None, :], (qblocks, QUERY_BLOCK, chosen_count * KEY_BLOCK)
    )
    lower_mask = jnp.broadcast_to(
        (jnp.arange(QUERY_BLOCK)[:, None] >= jnp.arange(QUERY_BLOCK)[None, :])[None],
        (qblocks, QUERY_BLOCK, QUERY_BLOCK),
    )
    full_mask = jnp.concatenate([far_mask, lower_mask], axis=2)
    scores = jnp.einsum(
        "bqngd,bknd->bngqk", block_queries, all_keys, preferred_element_type=jnp.float32
    ) * HEAD_DIM ** (-0.5)
    scores = jnp.where(full_mask[:, None, None], scores, -jnp.inf)
    row_max = jnp.max(scores, axis=-1, keepdims=True)
    weights = jnp.exp(scores - row_max)
    weights = (weights / jnp.sum(weights, axis=-1, keepdims=True)).astype(jnp.bfloat16)
    mixed_rows = (
        jnp.einsum("bngqk,bknd->bqngd", weights, all_values, preferred_element_type=jnp.float32)
        .astype(jnp.bfloat16)
        .reshape(tok_count, heads_here * HEAD_DIM)
    )
    terms = jnp.dot(mixed_rows, out_weight, preferred_element_type=jnp.float32)
    projected = lax.psum_scatter(
        terms.astype(jnp.bfloat16), "tp", scatter_dimension=1, tiled=True
    ).astype(jnp.float32)
    row_total = lax.psum(jnp.sum(projected * projected, axis=1), "tp")
    scale_rows = lax.rsqrt(row_total / D + norm_eps)
    result = (projected * scale_rows[:, None] * norm_gain[None, :]).astype(jnp.bfloat16)
    return result[None]


def solution(mesh):
    placed = (
        P("dp", "kv", None),
        P(None, "tp"),
        P(None, "tp"),
        P(None, "tp"),
        P("tp", None),
        P("tp"),
        P("dp", None, None),
        P("dp", None, None),
    )
    return jax.shard_map(
        body, mesh=mesh, in_specs=placed, out_specs=P("dp", "kv", "tp"), check_vma=False
    )
```

profile of v0, /device:TPU:27, one launch (start us, length us, event | category | flops | bytes accessed | tf_op | source)
XLA Modules:
  0.0 116.0 jit_solution(5359210719336470150)
XLA Ops:
  6.5 0.6 iota_compare_fusion.2
  7.2 2.3 %copy.52 = bf16[2048,128]{0,1:T(8,128)(2,1)} copy(bf16[2048,128]{1,0:T(8,128)(2,1)} %param.10) | data formatting | bytes 1048576 | tf_op args[2]
  9.5 0.4 multiply_cosine_fusion
  9.9 0.0 copy-start.4
  9.9 2.2 %fusion.13 = f32[768,2,64]{0,2,1:T(8,128)S(1)} fusion(bf16[2,64,2048]{2,1,0:T(8,128)(2,1)} %bitcast.97, bf16[1,768,2048]{2,1,0:T(8,128)(2,1)S(1)} %copy-done), kind=kOutput, calls=%fused_computation.22 | convolution fusion | flops 402653184 | bytes 4063232 | tf_op jit(solution)/shard_map/dot_general | solution.py:60
  12.2 0.1 subtract_convert_fusion.1
  12.3 0.6 copy-done.2
  12.9 0.0 copy-done.3
  12.9 1.1 copy.53
  14.0 1.2 %convert_element_type.47 = bf16[12,64,128]{2,1,0:T(8,128)(2,1)S(1)} reshape(bf16[768,2,64]{2,1,0:T(2,128)(2,1)} %copy.53) | data formatting | bytes 393216 | tf_op jit(solution)/shard_map/convert_element_type | solution.py:65
  15.3 0.1 copy.42
  15.3 0.1 reshape_squeeze.3
  15.4 0.5 broadcast_compare_fusion.1
  15.9 1.5 %convert_reduce_fusion = s32[4,24]{1,0:T(4,128)} fusion(s32[4,24]{1,0:T(4,128)S(1)} %reshape_squeeze.3, pred[24,24]{1,0:T(8,128)(4,1)} %iota_compare_fusion.2), kind=kLoop, calls=%fused_computation.49 | loop fusion | flops 9120 | bytes 1344 | tf_op jit(solution)/shard_map/vmap()/reduce_sum | solution.py:37
  17.4 0.8 copy.43
  18.2 0.1 broadcast_in_dim.34
  18.3 0.9 select_reduce_fusion
  19.1 0.1 copy.44
  19.2 0.1 reshape.212
  19.3 1.4 %gather_fusion.2 = bf16[24,64,128]{2,1,0:T(8,128)(2,1)} fusion(bf16[12,64,128]{2,1,0:T(8,128)(2,1)S(1)} %convert_element_type.47, s32[1024]{0:T(1024)S(1)} %pad_clamp_fusion.1), kind=kCustom, calls=%fused_computation.2 | custom fusion | bytes 786528 | tf_op jit(solution)/shard_map/gather | solution.py:90
  20.7 4.5 %all-to-all-start.1 = ((bf16[4,6,64,128]{3,2,1,0:T(8,128)(2,1)}), bf16[4,6,64,128]{3,2,1,0:T(8,128)(2,1)}, u32[]{:S(2)}, u32[]{:S(2)}) async-start(bf16[4,6,64,128]{3,2,1,0:T(8,128)(2,1)} %bitcast.95), calls=%async_computation.1 | async-start | bytes 786432 | tf_op jit(solution)/shard_map/all_to_all | solution.py:93
  25.2 0.8 broadcast_multiply_fusion
  26.0 0.1 copy.47
  26.1 0.1 eq.59
  26.1 0.1 copy.45
  26.3 0.7 ge.38
  26.9 0.1 copy.46
  27.0 0.1 mul.132
  27.1 4.0 %copy.57 = bf16[2048,512]{0,1:T(8,128)(2,1)} copy(bf16[2048,512]{1,0:T(8,128)(2,1)} %param.9) | data formatting | bytes 4194304 | tf_op args[1]
  31.1 4.6 %fusion.11 = f32[768,8,64]{0,2,1:T(8,128)} fusion(bf16[8,64,2048]{2,1,0:T(8,128)(2,1)} %bitcast.92, bf16[1,768,2048]{2,1,0:T(8,128)(2,1)S(1)} %copy-done), kind=kOutput, calls=%fused_computation.20 | convolution fusion | flops 1610612736 | bytes 6815744 | tf_op jit(solution)/shard_map/dot_general | solution.py:53
  35.7 1.0 fusion.20
  36.7 1.3 %gather_fusion = bf16[24,64,128]{2,1,0:T(8,128)(2,1)} fusion(bf16[12,64,128]{2,1,0:T(8,128)(2,1)S(1)} %bitcast.93, s32[1024]{0:T(1024)S(1)} %pad_clamp_fusion.1), kind=kCustom, calls=%fused_computation | custom fusion | bytes 786528 | tf_op jit(solution)/shard_map/gather | solution.py:91
  38.0 0.2 convert_reduce_fusion.1
  38.2 0.5 fusion.43
  38.7 2.5 %subtract_convert_fusion = (bf16[768,8,32]{0,2,1:T(8,128)(2,1)}, bf16[768,8,32]{0,2,1:T(8,128)(2,1)}) fusion(f32[768,8,64]{0,2,1:T(8,128)} %fusion.11, f32[768,32]{0,1:T(8,128)S(1)} %get-tuple-element.12, f32[768,32]{0,1:T(8,128)S(1)} %get-tuple-element.11), kind=kLoop, calls=%fused_computation.35 | loop fusion | flops 1572864 | bytes 2555904 | tf_op jit(solution)/shard_map/convert.3
  41.2 4.5 %all-to-all-start = ((bf16[4,6,64,128]{3,2,1,0:T(8,128)(2,1)}), bf16[4,6,64,128]{3,2,1,0:T(8,128)(2,1)}, u32[]{:S(2)}, u32[]{:S(2)}) async-start(bf16[4,6,64,128]{3,2,1,0:T(8,128)(2,1)} %bitcast.94), calls=%async_computation | async-start | bytes 786432 | tf_op jit(solution)/shard_map/all_to_all | solution.py:94
  45.7 0.7 fusion.29
  46.4 0.9 reshape.247
  47.3 0.1 copy.51
  47.4 0.1 broadcast_in_dim.37
  47.5 0.1 broadcast_in_dim.38
  47.6 2.2 %concatenate.37 = bf16[6,128,2,4,32]{1,0,4,3,2:T(8,128)(2,1)} reshape(bf16[768,8,32]{0,2,1:T(8,128)(2,1)} %get-tuple-element.7) | data formatting | bytes 786432 | tf_op jit(solution)/shard_map/concatenate | solution.py:24
  49.9 1.9 %copy.58 = bf16[6,128,2,4,32]{1,4,3,2,0:T(8,128)(2,1)} copy(bf16[6,128,2,4,32]{1,0,4,3,2:T(8,128)(2,1)} %concatenate.37) | data formatting | bytes 786432 | tf_op jit(solution)/shard_map/concatenate | solution.py:24
  51.7 2.2 %concatenate.38 = bf16[6,128,2,4,32]{1,0,4,3,2:T(8,128)(2,1)} reshape(bf16[768,8,32]{0,2,1:T(8,128)(2,1)} %get-tuple-element.8) | data formatting | bytes 786432 | tf_op jit(solution)/shard_map/concatenate | solution.py:24
  54.0 1.9 %copy.59 = bf16[6,128,2,4,32]{1,4,3,2,0:T(8,128)(2,1)} copy(bf16[6,128,2,4,32]{1,0,4,3,2:T(8,128)(2,1)} %concatenate.38) | data formatting | bytes 786432 | tf_op jit(solution)/shard_map/concatenate | solution.py:24
  55.8 0.9 copy.50
  56.8 0.3 broadcast_in_dim.39
  57.1 0.7 pad_add_fusion
  57.9 1.7 %copy_bitcast_fusion = (bf16[6,128,2,32]{1,3,2,0:T(8,128)(2,1)}, bf16[6,128,2,32]{1,3,2,0:T(8,128)(2,1)}) fusion(bf16[768,2,32]{0,2,1:T(8,128)(2,1)} %copy-done.2, bf16[768,2,32]{0,2,1:T(8,128)(2,1)} %copy-done.3), kind=kLoop, calls=%fused_computation.46 | loop fusion | bytes 393216 | tf_op jit(solution)/shard_map/concatenate | solution.py:24
  59.5 1.6 %gather_fusion.3 = bf16[24,64,128]{2,1,0:T(8,128)(2,1)S(1)} fusion(bf16[24,64,128]{2,1,0:T(8,128)(2,1)} %bitcast.14, s32[1024]{0:T(1024)S(1)} %pad_clamp_fusion), kind=kCustom, calls=%fused_computation.3 | custom fusion | bytes 786528 | tf_op jit(solution)/shard_map/gather | solution.py:97
  61.2 1.2 %reshape.208 = bf16[6,256,2,64]{3,2,1,0:T(2,128)(2,1)} reshape(bf16[24,64,128]{2,1,0:T(8,128)(2,1)S(1)} %gather_fusion.3) | data formatting | bytes 786432 | tf_op jit(solution)/shard_map/reshape | solution.py:100
  62.4 2.9 %copy.56 = bf16[6,256,2,64]{1,3,2,0:T(8,128)(2,1)} copy(bf16[6,256,2,64]{3,2,1,0:T(2,128)(2,1)} %reshape.208) | data formatting | bytes 786432 | tf_op jit(solution)/shard_map/reshape | solution.py:100
  65.2 1.6 %gather_fusion.1 = bf16[24,64,128]{2,1,0:T(8,128)(2,1)S(1)} fusion(bf16[24,64,128]{2,1,0:T(8,128)(2,1)} %bitcast.4, s32[1024]{0:T(1024)S(1)} %pad_clamp_fusion), kind=kCustom, calls=%fused_computation.1 | custom fusion | bytes 786528 | tf_op jit(solution)/shard_map/gather | solution.py:98
  66.9 1.2 %reshape.205 = bf16[6,256,2,64]{3,2,1,0:T(2,128)(2,1)} reshape(bf16[24,64,128]{2,1,0:T(8,128)(2,1)S(1)} %gather_fusion.1) | data formatting | bytes 786432 | tf_op jit(solution)/shard_map/reshape | solution.py:101
  68.1 2.2 %copy.49 = bf16[6,256,2,64]{1,3,2,0:T(8,128)(2,1)S(1)} copy(bf16[6,256,2,64]{3,2,1,0:T(2,128)(2,1)} %reshape.205) | data formatting | bytes 786432 | tf_op jit(solution)/shard_map/reshape | solution.py:101
  70.3 8.8 %fusion.38 = (f32[6,2,4,128]{3,2,1,0:T(4,128)}, f32[6,2,4,128,384]{3,4,2,1,0:T(8,128)}) fusion(pred[6,128,384]{1,2,0:T(8,128)(4,1)} %pad_add_fusion, bf16[6,128,2,4,32]{1,4,3,2,0:T(8,128)(2,1)} %copy.59, bf16[6,128,2,4,32]{1,4,3,2,0:T(8,128)(2,1)} %copy.58, bf16[6,128,2,32]{1,3,2,0:T(8,128)(2,1)} %get-tuple-element.15, ...), kind=kOutput, calls=%fused_computation.74 | convolution fusion | flops 314769792 | bytes 11132928 | tf_op jit(solution)/shard_map/sub | solution.py:124
  79.1 4.8 %fusion.19 = bf16[6,128,2,4,64]{1,4,3,2,0:T(8,128)(2,1)S(1)} fusion(f32[6,2,4,128,384]{3,4,2,1,0:T(8,128)} %get-tuple-element.14, f32[6,2,4,128]{3,2,1,0:T(4,128)} %get-tuple-element.13, bf16[6,128,2,64]{1,3,2,0:T(8,128)(2,1)} %copy.50, bf16[6,256,2,64]{1,3,2,0:T(8,128)(2,1)S(1)} %copy.49), kind=kOutput, calls=%fused_computation.28 | convolution fusion | flops 308281344 | bytes 10838016 | tf_op jit(solution)/shard_map/bngqk,bknd->bqngd/dot_general | solution.py:127
  83.9 0.6 copy.61
  84.5 3.5 %convolution_convert_fusion = bf16[768,2048]{1,0:T(8,128)(2,1)} fusion(bf16[512,2048]{1,0:T(8,128)(2,1)S(1)} %copy-done.7, bf16[64,8,6,128]{3,2,1,0:T(8,128)(2,1)S(1)} %bitcast.96), kind=kOutput, calls=%fused_computation.16 | convolution fusion | flops 1612185600 | bytes 6029312 | tf_op jit(solution)/shard_map/dot_general | solution.py:131
  88.0 0.0 reduce-scatter.2.cloned.1.call-update
  88.0 13.9 %reduce-scatter.2.cloned.1.call-done = bf16[768,1024]{1,0:T(8,128)(2,1)} async-done(((bf16[768,2048]{1,0:T(8,128)(2,1)}), bf16[768,1024]{1,0:T(8,128)(2,1)}) %reduce-scatter.2.cloned.1.call-update) | async-done | bytes 1572880 | tf_op jit(solution)/shard_map/reduce_scatter | solution.py:132
  101.9 1.8 %fusion.8 = f32[768]{0:T(1024)S(1)} fusion(bf16[768,1024]{1,0:T(8,128)(2,1)} %reduce-scatter.2.cloned.1.call-done), kind=kLoop, calls=%fused_computation.17 | loop fusion | flops 2358528 | bytes 1575936 | tf_op jit(solution)/shard_map/reduce_sum | solution.py:135
  103.7 2.5 %psum.7 = f32[768]{0:T(1024)S(1)} all-reduce(f32[768]{0:T(1024)S(1)} %fusion.8), channel_id=1, replica_groups=mesh['dp'=4,'kv'=4,'tp'=2] {'tp'}, use_global_device_ids=true, to_apply=%region_7.8 | all-reduce | flops 768 | bytes 6144 | tf_op jit(solution)/shard_map/psum | solution.py:135
  106.2 3.0 %fusion.17 = bf16[1,768,1024]{2,1,0:T(8,128)(2,1)} fusion(bf16[768,1024]{1,0:T(8,128)(2,1)} %reduce-scatter.2.cloned.1.call-done, f32[1024]{0:T(1024)S(1)} %copy-done.5, f32[768]{0:T(1024)S(1)} %add_rsqrt_fusion), kind=kLoop, calls=%fused_computation.26 | loop fusion | flops 3145728 | bytes 3152896 | tf_op jit(solution)/shard_map/broadcast_in_dim | solution.py:138
  (28 shorter events, 0.1 us)
Async XLA Ops:
  6.5 3.4 %copy-start = (bf16[1,768,2048]{2,1,0:T(8,128)(2,1)S(1)}, bf16[1,768,2048]{2,1,0:T(8,128)(2,1)}, u32[]{:S(2)}) copy-start(bf16[1,768,2048]{2,1,0:T(8,128)(2,1)} %param.8) | copy-start | bytes 9437188
  9.9 5.3 %copy-start.4 = (s32[1,24,4]{1,2,0:T(4,128)S(1)}, s32[1,24,4]{1,2,0:T(4,128)}, u32[]{:S(2)}) copy-start(s32[1,24,4]{1,2,0:T(4,128)} %param.14) | copy-start | bytes 1156
  12.2 0.6 copy-start.2
  12.2 0.7 copy-start.3
  20.7 20.5 %all-to-all-start.1 = ((bf16[4,6,64,128]{3,2,1,0:T(8,128)(2,1)}), bf16[4,6,64,128]{3,2,1,0:T(8,128)(2,1)}, u32[]{:S(2)}, u32[]{:S(2)}) async-start(bf16[4,6,64,128]{3,2,1,0:T(8,128)(2,1)} %bitcast.95), calls=%async_computation.1 | async-start | bytes 786432 | tf_op jit(solution)/shard_map/all_to_all | solution.py:93
  31.1 4.6 %copy-start.8 = (bf16[2048,128]{1,0:T(8,128)(2,1)S(1)}, bf16[2048,128]{1,0:T(8,128)(2,1)}, u32[]{:S(2)}) copy-start(bf16[2048,128]{1,0:T(8,128)(2,1)} %param.11) | copy-start | bytes 1572868
  38.7 8.6 %copy-start.6 = (pred[6,4]{0,1:T(4,128)(4,1)S(1)}, pred[6,4]{0,1:T(4,128)(4,1)}, u32[]{:S(2)}) copy-start(pred[6,4]{0,1:T(4,128)(4,1)} %fusion.43) | copy-start | bytes 76
  41.2 24.0 %all-to-all-start = ((bf16[4,6,64,128]{3,2,1,0:T(8,128)(2,1)}), bf16[4,6,64,128]{3,2,1,0:T(8,128)(2,1)}, u32[]{:S(2)}, u32[]{:S(2)}) async-start(bf16[4,6,64,128]{3,2,1,0:T(8,128)(2,1)} %bitcast.94), calls=%async_computation | async-start | bytes 786432 | tf_op jit(solution)/shard_map/all_to_all | solution.py:94
  45.7 56.2 %reduce-scatter.2.cloned.1.call-start = ((), (), s32[]{:S(2)}) async-start(), calls=%async_computation.3 | async-start | bytes 4718592 | tf_op jit(solution)/shard_map/reduce_scatter | solution.py:132
  47.3 8.5 %copy-start.1 = (bf16[6,128,2,64]{3,2,1,0:T(2,128)(2,1)S(1)}, bf16[6,128,2,64]{3,2,1,0:T(2,128)(2,1)}, u32[]{:S(2)}) copy-start(bf16[6,128,2,64]{3,2,1,0:T(2,128)(2,1)} %reshape.247) | copy-start | bytes 589828
  79.1 5.4 %copy-start.7 = (bf16[512,2048]{1,0:T(8,128)(2,1)S(1)}, bf16[512,2048]{1,0:T(8,128)(2,1)}, u32[]{:S(2)}) copy-start(bf16[512,2048]{1,0:T(8,128)(2,1)} %param.12) | copy-start | bytes 6291460
  88.0 18.2 %copy-start.5 = (f32[1024]{0:T(1024)S(1)}, f32[1024]{0:T(1024)}, u32[]{:S(2)}) copy-start(f32[1024]{0:T(1024)} %param.13) | copy-start | bytes 12292
Sparse Core Ops, SparseCore 0:
  88.2 13.7 reduce-scatter.1
where the time goes:
time: 118 us; the launch traced here: 116 us
  local copies, waits for them, and re-layouts  37.9 us (32%)
  matrix products  25 us (21%)
  other arithmetic  14.1 us (12%)
  waiting for transfers between devices  13.9 us (12%)
  between operations  13.6 us (12%)
  starting transfers between devices  9.07 us (8%)
  blocking collectives  2.48 us (2%)
    reduce_scatter x1, waiting for transfers between devices, body(): lax.psum_scatter(terms.astype(jnp.bfloat16), 'tp', scatter_dimension=1, t...  13.9 us
    concatenate x6, local copies, waits for them, and re-layouts, rotate(): jnp.concatenate([first_half * cosine - second_half * sine_part, second_ha...  11 us
    sub x1, matrix products, body(): weights = jnp.exp(scores - row_max)  8.85 us
    unnamed x22, local copies, waits for them, and re-layouts  7.87 us
    dot_general x1, matrix products, body(): jnp.einsum('bngqk,bknd->bqngd', weights, all_values, preferred_element_ty...  4.79 us
    dot_general x1, matrix products, body(): jnp.dot(row_data, query_weight, preferred_element_type=jnp.float32)  4.62 us
    all_to_all x1, starting transfers between devices, body(): lax.all_to_all(send_values, 'kv', split_axis=0, concat_axis=0, tiled=True)  4.53 us
    all_to_all x1, starting transfers between devices, body(): lax.all_to_all(send_keys, 'kv', split_axis=0, concat_axis=0, tiled=True)  4.53 us
  transfers between devices with their start and end apart: 3, of which 1 were waited for; matrix products, arithmetic and copies ran while one was open for 31% of the time, Pallas kernels for 0%

commit v1 on v0

v1 whole, which is shorter than its diff:
```python
import functools

import jax
import jax.numpy as jnp
from jax import lax
from jax.experimental import pallas as pl
from jax.experimental.pallas import tpu as pltpu
from jax.sharding import PartitionSpec as P

HEAD_DIM = 64
QUERY_BLOCK = 128
KEY_BLOCK = 64
LANES = 128
ROWS = 256
COLS = 256

rope_base = 10000.0
norm_eps = 1e-06
MESH = pl.DeviceIdType.MESH


def turn(u, cosine, sine):
    lane = lax.broadcasted_iota(jnp.int32, u.shape, 1)
    half = HEAD_DIM // 2
    swapped = jnp.where(
        lane % HEAD_DIM < half, pltpu.roll(u, LANES - half, 1), pltpu.roll(u, half, 1)
    )
    return u * cosine + swapped * sine


def spread(pair, head):
    wide = pair.astype(jnp.float32)
    swapped = pltpu.roll(wide, HEAD_DIM, 1)
    low = lax.broadcasted_iota(jnp.int32, wide.shape, 1) < HEAD_DIM
    in_low, in_high = (wide, swapped) if head == 0 else (swapped, wide)
    return jnp.concatenate(
        [jnp.where(low, in_low, 0.0), jnp.where(low, 0.0, in_high)], axis=0
    ).astype(jnp.bfloat16)


def kernel(
    devices, owner_ref, part_ref, tok, wq, wk, wv, ow, gain, cosine, sine, out,
    kv, send, pool, queries, mix, mix_other, ow_other, proj, ss, ss_other,
    kv_send, kv_recv, ow_sems, mix_send, mix_recv, ss_sems,
):
    me = lax.axis_index("kv")
    core = lax.axis_index("tp")
    other = 1 - core
    tokens = tok.shape[0]
    qblocks = tokens // QUERY_BLOCK
    chosen = owner_ref.shape[1]
    half = ow_other.shape[1]
    row_steps = tokens // ROWS
    per_q = QUERY_BLOCK // KEY_BLOCK

    barrier = pltpu.get_barrier_semaphore()

    @pl.loop(0, devices)
    def _(j):
        @pl.when(j != me)
        def _():
            pl.semaphore_signal(barrier, inc=1, device_id={"kv": j}, device_id_type=MESH)

    pl.semaphore_signal(barrier, inc=1, device_id={"tp": other}, device_id_type=MESH)

    @pl.loop(0, row_steps)
    def _(r):
        rows = pl.ds(pl.multiple_of(r * ROWS, ROWS), ROWS)
        both = jnp.dot(
            tok[rows, :],
            jnp.concatenate([wk[...], wv[...]], axis=1),
            preferred_element_type=jnp.float32,
        )
        keys = turn(both[:, :LANES], cosine[rows, :], sine[rows, :])
        joined = jnp.concatenate([keys, both[:, LANES:]], axis=1).astype(jnp.bfloat16)
        blocks = ROWS // KEY_BLOCK
        kv[pl.ds(r * blocks, blocks)] = joined.reshape(blocks, KEY_BLOCK, 2 * LANES)

    pl.semaphore_wait(barrier, devices)

    def wanted(dst, q):
        row = dst * qblocks + q
        return sum(
            jnp.where(owner_ref[row, s] == me, part_ref[row, s], 0) for s in range(chosen)
        )

    def kv_copy(src, dst):
        return pltpu.make_async_remote_copy(
            src_ref=send.at[pl.ds(dst * qblocks, qblocks)],
            dst_ref=pool.at[pl.ds(src * qblocks, qblocks)],
            send_sem=kv_send.at[dst],
            recv_sem=kv_recv.at[src],
            device_id={"kv": dst},
            device_id_type=MESH,
        )

    @pl.loop(0, devices)
    def _(dst):
        @pl.when(dst > me)
        def _():
            for q in range(qblocks):
                send[pl.ds(dst * qblocks + q, 1)] = kv[pl.ds(wanted(dst, q), 1)]
            kv_copy(me, dst).start()

        @pl.when(dst == me)
        def _():
            for q in range(qblocks):
                pool[pl.ds(me * qblocks + q, 1)] = kv[pl.ds(wanted(me, q), 1)]

    ow_copy = pltpu.make_async_remote_copy(
        src_ref=ow.at[:, pl.ds(pl.multiple_of(other * half, half), half)],
        dst_ref=ow_other,
        send_sem=ow_sems.at[0],
        recv_sem=ow_sems.at[1],
        device_id={"tp": other},
        device_id_type=MESH,
    )
    ow_copy.start()

    @pl.loop(0, row_steps)
    def _(r):
        rows = pl.ds(pl.multiple_of(r * ROWS, ROWS), ROWS)
        for c in range(wq.shape[1] // COLS):
            part = jnp.dot(
                tok[rows, :], wq[:, c * COLS : (c + 1) * COLS], preferred_element_type=jnp.float32
            )
            for k in range(COLS // LANES):
                at = c * COLS + k * LANES
                queries[rows, at : at + LANES] = turn(
                    part[:, k * LANES : (k + 1) * LANES], cosine[rows, :], sine[rows, :]
                ).astype(jnp.bfloat16)

    @pl.loop(0, devices)
    def _(src):
        @pl.when(src < me)
        def _():
            kv_copy(src, me).wait_recv()

    kv_heads = wk.shape[1] // HEAD_DIM
    slices = wq.shape[1] // LANES // kv_heads
    key_count = chosen * KEY_BLOCK + QUERY_BLOCK

    def mix_copy(b):
        rows = pl.ds(pl.multiple_of(b * QUERY_BLOCK, QUERY_BLOCK), QUERY_BLOCK)
        return pltpu.make_async_remote_copy(
            src_ref=mix.at[rows],
            dst_ref=mix_other.at[rows],
            send_sem=mix_send.at[b],
            recv_sem=mix_recv.at[b],
            device_id={"tp": other},
            device_id_type=MESH,
        )

    @pl.loop(0, qblocks)
    def _(b):
        row = me * qblocks + b
        rows = pl.ds(pl.multiple_of(b * QUERY_BLOCK, QUERY_BLOCK), QUERY_BLOCK)
        pieces = []
        lane = lax.broadcasted_iota(jnp.int32, (1, chosen * KEY_BLOCK), 1) // KEY_BLOCK
        far = jnp.zeros((1, chosen * KEY_BLOCK), jnp.float32)
        for s in range(chosen):
            owner = owner_ref[row, s]
            at = jnp.where(owner >= 0, owner * qblocks + b, 0)
            pieces.append(pool[pl.ds(at, 1)].reshape(KEY_BLOCK, 2 * LANES))
            far = jnp.where(lane == s, jnp.where(owner >= 0, 0.0, -jnp.inf), far)
        pieces.append(kv[pl.ds(b * per_q, per_q)].reshape(QUERY_BLOCK, 2 * LANES))
        near = jnp.where(
            lax.broadcasted_iota(jnp.int32, (slices * QUERY_BLOCK, QUERY_BLOCK), 0) % QUERY_BLOCK
            >= lax.broadcasted_iota(jnp.int32, (slices * QUERY_BLOCK, QUERY_BLOCK), 1),
            0.0,
            -jnp.inf,
        )
        bias = jnp.concatenate(
            [jnp.broadcast_to(far, (slices * QUERY_BLOCK, chosen * KEY_BLOCK)), near], axis=1
        )
        both = jnp.concatenate(pieces, axis=0)
        for n in range(kv_heads):
            q = jnp.concatenate(
                [
                    queries[rows, (n * slices + m) * LANES : (n * slices + m + 1) * LANES]
                    for m in range(slices)
                ],
                axis=0,
            )
            scores = lax.dot_general(
                q,
                spread(both[:, :LANES], n),
                (((1,), (1,)), ((), ())),
                preferred_element_type=jnp.float32,
            )
            probs = []
            for side in range(2):
                s = scores[:, side * key_count : (side + 1) * key_count] * HEAD_DIM**-0.5 + bias
                e = jnp.exp(s - jnp.max(s, axis=1, keepdims=True))
                probs.append((e * (1.0 / jnp.sum(e, axis=1, keepdims=True))).astype(jnp.bfloat16))
            mixed = jnp.dot(
                jnp.concatenate(probs, axis=1),
                spread(both[:, LANES:], n),
                preferred_element_type=jnp.float32,
            ).astype(jnp.bfloat16)
            for m in range(slices):
                at = (n * slices + m) * LANES
                mix[rows, at : at + LANES] = mixed[m * QUERY_BLOCK : (m + 1) * QUERY_BLOCK]
        mix_copy(b).start()

    ow_copy.wait_recv()

    @pl.loop(0, qblocks)
    def _(b):
        mix_copy(b).wait_recv()

    @pl.loop(0, row_steps)
    def _(r):
        rows = pl.ds(pl.multiple_of(r * ROWS, ROWS), ROWS)
        total = jnp.zeros((ROWS, LANES), jnp.float32)
        for c in range(half // COLS):
            mine = jnp.dot(
                mix[rows, :],
                ow[:, pl.ds(pl.multiple_of(core * half + c * COLS, COLS), COLS)],
                preferred_element_type=jnp.float32,
            ).astype(jnp.bfloat16)
            theirs = jnp.dot(
                mix_other[rows, :],
                ow_other[:, c * COLS : (c + 1) * COLS],
                preferred_element_type=jnp.float32,
            ).astype(jnp.bfloat16)
            added = mine.astype(jnp.float32) + theirs.astype(jnp.float32)
            proj[rows, c * COLS : (c + 1) * COLS] = added
            for k in range(COLS // LANES):
                piece = added[:, k * LANES : (k + 1) * LANES]
                total = total + piece * piece
        for k in range(ROWS // LANES):
            ss[r * (ROWS // LANES) + k] = jnp.sum(
                total[k * LANES : (k + 1) * LANES].T, axis=0, keepdims=True
            )

    ss_copy = pltpu.make_async_remote_copy(
        src_ref=ss,
        dst_ref=ss_other,
        send_sem=ss_sems.at[0],
        recv_sem=ss_sems.at[1],
        device_id={"tp": other},
        device_id_type=MESH,
    )
    ss_copy.start()

    @pl.loop(0, devices)
    def _(dst):
        @pl.when(dst > me)
        def _():
            kv_copy(me, dst).wait_send()

    ow_copy.wait_send()

    @pl.loop(0, qblocks)
    def _(b):
        mix_copy(b).wait_send()

    ss_copy.wait()

    @pl.loop(0, qblocks)
    def _(b):
        rows = pl.ds(pl.multiple_of(b * LANES, LANES), LANES)
        scale = lax.rsqrt((ss[b] + ss_other[b]) / (2 * half) + norm_eps)
        scale = jnp.broadcast_to(scale, (LANES, LANES)).T
        for c in range(half // LANES):
            at = slice(c * LANES, (c + 1) * LANES)
            out[rows, at] = (proj[rows, at] * scale * gain[:, at]).astype(jnp.bfloat16)


def body(
    tokens, query_weight, key_weight, value_weight, out_weight, norm_gain, chosen_owner, chosen_part
):
    row_data = tokens[0]
    count = row_data.shape[0]
    devices = lax.axis_size("kv")
    qblocks = count // QUERY_BLOCK
    positions = lax.axis_index("kv") * count + jnp.arange(count, dtype=jnp.int32)
    half_dim = HEAD_DIM // 2
    frequency = rope_base ** (-jnp.arange(half_dim, dtype=jnp.float32) / half_dim)
    angles = positions.astype(jnp.float32)[:, None] * frequency
    cosine, sine = jnp.cos(angles), jnp.sin(angles)
    cosine = jnp.concatenate([cosine] * (LANES // half_dim), axis=1)
    sine = jnp.concatenate([-sine, sine] * (LANES // HEAD_DIM), axis=1)
    heads_width = query_weight.shape[1]
    half = norm_gain.shape[0]
    vmem = pl.BlockSpec(memory_space=pltpu.VMEM)
    smem = pl.BlockSpec(memory_space=pltpu.SMEM)
    bf16, f32 = jnp.bfloat16, jnp.float32
    result = pl.pallas_call(
        functools.partial(kernel, devices),
        out_shape=jax.ShapeDtypeStruct((count, half), bf16),
        in_specs=[smem] * 2 + [vmem] * 8,
        out_specs=vmem,
        scratch_shapes=[
            pltpu.VMEM((count // KEY_BLOCK, KEY_BLOCK, 2 * LANES), bf16),
            pltpu.VMEM((devices * qblocks, KEY_BLOCK, 2 * LANES), bf16),
            pltpu.VMEM((devices * qblocks, KEY_BLOCK, 2 * LANES), bf16),
            pltpu.VMEM((count, heads_width), bf16),
            pltpu.VMEM((count, heads_width), bf16),
            pltpu.VMEM((count, heads_width), bf16),
            pltpu.VMEM((out_weight.shape[0], half), bf16),
            pltpu.VMEM((count, half), f32),
            pltpu.VMEM((qblocks, 1, LANES), f32),
            pltpu.VMEM((qblocks, 1, LANES), f32),
            pltpu.SemaphoreType.DMA((devices,)),
            pltpu.SemaphoreType.DMA((devices,)),
            pltpu.SemaphoreType.DMA((2,)),
            pltpu.SemaphoreType.DMA((qblocks,)),
            pltpu.SemaphoreType.DMA((qblocks,)),
            pltpu.SemaphoreType.DMA((2,)),
        ],
        compiler_params=pltpu.CompilerParams(
            collective_id=0, has_side_effects=True, vmem_limit_bytes=60 * 1024 * 1024
        ),
    )(
        chosen_owner[0], chosen_part[0], row_data, query_weight, key_weight, value_weight,
        out_weight, norm_gain[None], cosine, sine,
    )
    return result[None]


def solution(mesh):
    placed = (
        P("dp", "kv", None),
        P(None, "tp"),
        P(None, "tp"),
        P(None, "tp"),
        P("tp", None),
        P("tp"),
        P("dp", None, None),
        P("dp", None, None),
    )
    return jax.shard_map(
        body, mesh=mesh, in_specs=placed, out_specs=P("dp", "kv", "tp"), check_vma=False
    )
```

time: 118 us -> 47.2 us (0.40); the launches traced: 116 us -> 47 us
  Pallas kernels: 0 us -> 38.6 us
  local copies, waits for them, and re-layouts: 37.9 us -> 5.38 us
  matrix products: 25 us -> 0 us
  waiting for transfers between devices: 13.9 us -> 0 us
  between operations: 13.6 us -> 0.02 us
  other arithmetic: 14.1 us -> 3.01 us
  starting transfers between devices: 9.07 us -> 0 us
  blocking collectives: 2.48 us -> 0 us
    pallas_call x0 -> x1, Pallas kernels: none -> 38.6 us  [body(): pl.pallas_call(functools.partial(kernel, devices), out_shape=jax.ShapeDty...]
    dot_general x5 -> x0, matrix products: 16.1 us -> none  [the longest x1 4.79 us: body(): jnp.einsum('bngqk,bknd->bqngd', weights, all_values, preferred_element_ty...]
    reduce_scatter x1 -> x0, waiting for transfers between devices: 13.9 us -> none  [body(): lax.psum_scatter(terms.astype(jnp.bfloat16), 'tp', scatter_dimension=1, t...]
    concatenate x6 -> x0, local copies, waits for them, and re-layouts: 11 us -> none  [rotate(): jnp.concatenate([first_half * cosine - second_half * sine_part, second_ha...]
    reshape x6 -> x0, local copies, waits for them, and re-layouts: 9.35 us -> none  [the longest x2 4.08 us: body(): picked_keys.reshape(qblocks, chosen_count * KEY_BLOCK, kv_here, HEAD_DIM)]
    all_to_all x2 -> x0, starting transfers between devices: 9.06 us -> none  [the longest x1 4.53 us: body(): lax.all_to_all(send_values, 'kv', split_axis=0, concat_axis=0, tiled=True)]
    sub x1 -> x0, matrix products: 8.85 us -> none  [body(): weights = jnp.exp(scores - row_max)]
    gather x4 -> x0, local copies, waits for them, and re-layouts: 5.93 us -> none  [the longest x1 1.62 us: body(): got_values.reshape(devices * qblocks, KEY_BLOCK, kv_width)[slot_index]]
  transfers between devices with their start and end apart: 3 -> 0, of which waited for: 1 -> 0; matrix products, arithmetic and copies ran while one was open for 31% -> 0% of each run, Pallas kernels for 0% -> 0%
where the time goes in v1:
time: 47.2 us; the launch traced here: 47 us
  Pallas kernels  38.6 us (82%)
  local copies, waits for them, and re-layouts  5.38 us (11%)
  other arithmetic  3.01 us (6%)
    pallas_call x1, Pallas kernels, body(): pl.pallas_call(functools.partial(kernel, devices), out_shape=jax.ShapeDty...  38.6 us
    unnamed x1, local copies, waits for them, and re-layouts  2.67 us
    concatenate x1, other arithmetic, body(): cosine = jnp.concatenate([cosine] * (LANES // half_dim), axis=1)  1.56 us
    neg x1, other arithmetic, body(): sine = jnp.concatenate([-sine, sine] * (LANES // HEAD_DIM), axis=1)  1.44 us
    squeeze x1, local copies, waits for them, and re-layouts, body(): chosen_owner[0]  1.36 us
    squeeze x1, local copies, waits for them, and re-layouts, body(): chosen_part[0]  1.36 us

profile of v1, /device:TPU:27, one launch (start us, length us, event | category | flops | bytes accessed | tf_op | source)
XLA Modules:
  0.0 47.0 jit_solution(1674891072785265254)
XLA Ops:
  0.0 1.4 %copy.12.owner_ref = s32[24,4]{1,0:T(8,128)} copy(s32[24,4]{0,1:T(4,128)} %bitcast.8) | data formatting | bytes 768 | tf_op jit(solution)/shard_map/squeeze | solution.py:317
  1.4 1.4 %copy.13.part_ref = s32[24,4]{1,0:T(8,128)} copy(s32[24,4]{0,1:T(4,128)} %bitcast.9) | data formatting | bytes 768 | tf_op jit(solution)/shard_map/squeeze | solution.py:317
  2.7 1.4 %fusion = (f32[768,32]{1,0:T(8,128)S(1)}, f32[768,32]{1,0:T(8,128)S(1)}, f32[768,32]{1,0:T(8,128)S(1)}) fusion(f32[32]{0:T(128)S(1)} %multiply_power_fusion, f32[768]{0:T(1024)S(1)} %add_convert_fusion), kind=kLoop, calls=%fused_computation.4 | loop fusion | flops 49152 | bytes 298112 | tf_op jit(solution)/shard_map/neg | solution.py:284
  4.2 1.6 %pad_maximum_fusion = (f32[768,128]{1,0:T(8,128)}, f32[768,128]{1,0:T(8,128)}) fusion(f32[768,32]{1,0:T(8,128)S(1)} %get-tuple-element.7, f32[768,32]{1,0:T(8,128)S(1)} %get-tuple-element.6, f32[768,32]{1,0:T(8,128)S(1)} %get-tuple-element.5), kind=kLoop, calls=%fused_computation.2 | loop fusion | flops 589824 | bytes 1081344 | tf_op jit(solution)/shard_map/concatenate | solution.py:283
  5.7 38.6 %shard_map.82 = bf16[768,1024]{1,0:T(8,128)(2,1)} custom-call(s32[24,4]{1,0:T(8,128)} %copy.12.owner_ref, s32[24,4]{1,0:T(8,128)} %copy.13.part_ref, bf16[768,2048]{1,0:T(8,128)(2,1)} %bitcast.6, bf16[2048,512]{1,0:T(8,128)(2,1)} %wq.1, bf16[2048,128]{1,0:T(8,128)(2,1)} %wk.1, bf16[2048,128]{1,0:T(8,128)(2,1)} %wv.1, bf16[512,2048]{1,0:T(8,128)(2,1)} %ow.1, ...), custom_call_target="tpu_custom_call" | custom-call | tf_op jit(solution)/shard_map/pallas_call | solution.py:290
  44.4 2.7 %copy.15 = bf16[1,768,1024]{2,1,0:T(8,128)(2,1)} copy(bf16[1,768,1024]{2,1,0:T(8,128)(2,1)} %bitcast.5) | data formatting | bytes 3145728
  (2 shorter events, 0.0 us)

commit v2 on v1

--- a/solution.py
+++ b/solution.py
@@ -39,7 +39,7 @@
 
 
 def kernel(
-    devices, owner_ref, part_ref, tok, wq, wk, wv, ow, gain, cosine, sine, out,
+    devices, ids_ref, tok, wq, wk, wv, ow, gain, cosine, sine, out,
     kv, send, pool, queries, mix, mix_other, ow_other, proj, ss, ss_other,
     kv_send, kv_recv, ow_sems, mix_send, mix_recv, ss_sems,
 ):
@@ -48,7 +48,8 @@
     other = 1 - core
     tokens = tok.shape[0]
     qblocks = tokens // QUERY_BLOCK
-    chosen = owner_ref.shape[1]
+    chosen = ids_ref.shape[1]
+    held = tokens // KEY_BLOCK
     half = ow_other.shape[1]
     row_steps = tokens // ROWS
     per_q = QUERY_BLOCK // KEY_BLOCK
@@ -78,34 +79,42 @@
 
     pl.semaphore_wait(barrier, devices)
 
+    def place(src, row, s):
+        at = ids_ref[row, s] - src * held
+        return jnp.logical_and(at >= 0, at < held), at
+
     def wanted(dst, q):
-        row = dst * qblocks + q
-        return sum(
-            jnp.where(owner_ref[row, s] == me, part_ref[row, s], 0) for s in range(chosen)
-        )
-
-    def kv_copy(src, dst):
+        found = [place(me, dst * qblocks + q, s) for s in range(chosen)]
+        return sum(jnp.where(here, at, 0) for here, at in found)
+
+    def kv_copy(src, dst, to, q):
         return pltpu.make_async_remote_copy(
-            src_ref=send.at[pl.ds(dst * qblocks, qblocks)],
-            dst_ref=pool.at[pl.ds(src * qblocks, qblocks)],
-            send_sem=kv_send.at[dst],
-            recv_sem=kv_recv.at[src],
-            device_id={"kv": dst},
+            src_ref=send.at[pl.ds(q * devices + dst, 1)],
+            dst_ref=pool.at[pl.ds(q * devices + src, 1)],
+            send_sem=kv_send.at[q, dst],
+            recv_sem=kv_recv.at[q, src],
+            device_id={"kv": to},
             device_id_type=MESH,
         )
 
-    @pl.loop(0, devices)
-    def _(dst):
-        @pl.when(dst > me)
-        def _():
-            for q in range(qblocks):
-                send[pl.ds(dst * qblocks + q, 1)] = kv[pl.ds(wanted(dst, q), 1)]
-            kv_copy(me, dst).start()
-
-        @pl.when(dst == me)
-        def _():
-            for q in range(qblocks):
-                pool[pl.ds(me * qblocks + q, 1)] = kv[pl.ds(wanted(me, q), 1)]
+    @pl.loop(0, qblocks)
+    def _(q):
+        @pl.loop(0, devices)
+        def _(dst):
+            @pl.when(dst > me)
+            def _():
+                send[pl.ds(q * devices + dst, 1)] = kv[pl.ds(wanted(dst, q), 1)]
+                kv_copy(me, dst, dst, q).start()
+
+            @pl.when(dst == me)
+            def _():
+                pool[pl.ds(q * devices + me, 1)] = kv[pl.ds(wanted(me, q), 1)]
+
+            @pl.when(dst > me)
+            def _():
+                pool[pl.ds(q * devices + dst, 1)] = jnp.zeros(
+                    (1, KEY_BLOCK, 2 * LANES), jnp.bfloat16
+                )
 
     ow_copy = pltpu.make_async_remote_copy(
         src_ref=ow.at[:, pl.ds(pl.multiple_of(other * half, half), half)],
@@ -130,15 +139,9 @@
                     part[:, k * LANES : (k + 1) * LANES], cosine[rows, :], sine[rows, :]
                 ).astype(jnp.bfloat16)
 
-    @pl.loop(0, devices)
-    def _(src):
-        @pl.when(src < me)
-        def _():
-            kv_copy(src, me).wait_recv()
-
     kv_heads = wk.shape[1] // HEAD_DIM
     slices = wq.shape[1] // LANES // kv_heads
-    key_count = chosen * KEY_BLOCK + QUERY_BLOCK
+    key_count = devices * KEY_BLOCK + QUERY_BLOCK
 
     def mix_copy(b):
         rows = pl.ds(pl.multiple_of(b * QUERY_BLOCK, QUERY_BLOCK), QUERY_BLOCK)
@@ -151,18 +154,22 @@
             device_id_type=MESH,
         )
 
-    @pl.loop(0, qblocks)
-    def _(b):
+    def attend(b):
         row = me * qblocks + b
+
+        @pl.loop(0, devices)
+        def _(src):
+            @pl.when(src < me)
+            def _():
+                kv_copy(src, src, src, b).wait_recv()
+
         rows = pl.ds(pl.multiple_of(b * QUERY_BLOCK, QUERY_BLOCK), QUERY_BLOCK)
-        pieces = []
-        lane = lax.broadcasted_iota(jnp.int32, (1, chosen * KEY_BLOCK), 1) // KEY_BLOCK
-        far = jnp.zeros((1, chosen * KEY_BLOCK), jnp.float32)
-        for s in range(chosen):
-            owner = owner_ref[row, s]
-            at = jnp.where(owner >= 0, owner * qblocks + b, 0)
-            pieces.append(pool[pl.ds(at, 1)].reshape(KEY_BLOCK, 2 * LANES))
-            far = jnp.where(lane == s, jnp.where(owner >= 0, 0.0, -jnp.inf), far)
+        pieces = [pool[pl.ds(b * devices, devices)].reshape(devices * KEY_BLOCK, 2 * LANES)]
+        lane = lax.broadcasted_iota(jnp.int32, (1, devices * KEY_BLOCK), 1) // KEY_BLOCK
+        far = jnp.full((1, devices * KEY_BLOCK), -jnp.inf, jnp.float32)
+        for src in range(devices):
+            named = sum(jnp.where(place(src, row, s)[0], 1, 0) for s in range(chosen))
+            far = jnp.where(lane == src, jnp.where(named > 0, 0.0, -jnp.inf), far)
         pieces.append(kv[pl.ds(b * per_q, per_q)].reshape(QUERY_BLOCK, 2 * LANES))
         near = jnp.where(
             lax.broadcasted_iota(jnp.int32, (slices * QUERY_BLOCK, QUERY_BLOCK), 0) % QUERY_BLOCK
@@ -171,7 +178,7 @@
             -jnp.inf,
         )
         bias = jnp.concatenate(
-            [jnp.broadcast_to(far, (slices * QUERY_BLOCK, chosen * KEY_BLOCK)), near], axis=1
+            [jnp.broadcast_to(far, (slices * QUERY_BLOCK, devices * KEY_BLOCK)), near], axis=1
         )
         both = jnp.concatenate(pieces, axis=0)
         for n in range(kv_heads):
@@ -203,14 +210,11 @@
                 mix[rows, at : at + LANES] = mixed[m * QUERY_BLOCK : (m + 1) * QUERY_BLOCK]
         mix_copy(b).start()
 
-    ow_copy.wait_recv()
-
-    @pl.loop(0, qblocks)
-    def _(b):
-        mix_copy(b).wait_recv()
-
-    @pl.loop(0, row_steps)
-    def _(r):
+    blocks_in = ROWS // QUERY_BLOCK
+
+    def project(r):
+        for k in range(blocks_in):
+            mix_copy(r * blocks_in + k).wait_recv()
         rows = pl.ds(pl.multiple_of(r * ROWS, ROWS), ROWS)
         total = jnp.zeros((ROWS, LANES), jnp.float32)
         for c in range(half // COLS):
@@ -234,6 +238,20 @@
                 total[k * LANES : (k + 1) * LANES].T, axis=0, keepdims=True
             )
 
+    ow_copy.wait_recv()
+
+    @pl.loop(0, row_steps)
+    def _(r):
+        @pl.loop(0, blocks_in)
+        def _(k):
+            attend(r * blocks_in + k)
+
+        @pl.when(r > 0)
+        def _():
+            project(r - 1)
+
+    project(row_steps - 1)
+
     ss_copy = pltpu.make_async_remote_copy(
         src_ref=ss,
         dst_ref=ss_other,
@@ -244,11 +262,13 @@
     )
     ss_copy.start()
 
-    @pl.loop(0, devices)
-    def _(dst):
-        @pl.when(dst > me)
-        def _():
-            kv_copy(me, dst).wait_send()
+    @pl.loop(0, qblocks)
+    def _(q):
+        @pl.loop(0, devices)
+        def _(dst):
+            @pl.when(dst > me)
+            def _():
+                kv_copy(me, dst, dst, q).wait_send()
 
     ow_copy.wait_send()
 
@@ -277,11 +297,14 @@
     qblocks = count // QUERY_BLOCK
     positions = lax.axis_index("kv") * count + jnp.arange(count, dtype=jnp.int32)
     half_dim = HEAD_DIM // 2
-    frequency = rope_base ** (-jnp.arange(half_dim, dtype=jnp.float32) / half_dim)
+    lane = jnp.arange(LANES, dtype=jnp.int32)
+    frequency = rope_base ** (-(lane % half_dim).astype(jnp.float32) / half_dim)
     angles = positions.astype(jnp.float32)[:, None] * frequency
-    cosine, sine = jnp.cos(angles), jnp.sin(angles)
-    cosine = jnp.concatenate([cosine] * (LANES // half_dim), axis=1)
-    sine = jnp.concatenate([-sine, sine] * (LANES // HEAD_DIM), axis=1)
+    cosine = jnp.cos(angles)
+    sine = jnp.where(lane % HEAD_DIM < half_dim, -1.0, 1.0) * jnp.sin(angles)
+    ids = jnp.where(
+        chosen_owner[0] >= 0, chosen_owner[0] * (count // KEY_BLOCK) + chosen_part[0], -1
+    )
     heads_width = query_weight.shape[1]
     half = norm_gain.shape[0]
     vmem = pl.BlockSpec(memory_space=pltpu.VMEM)
@@ -290,7 +313,7 @@
     result = pl.pallas_call(
         functools.partial(kernel, devices),
         out_shape=jax.ShapeDtypeStruct((count, half), bf16),
-        in_specs=[smem] * 2 + [vmem] * 8,
+        in_specs=[smem] + [vmem] * 8,
         out_specs=vmem,
         scratch_shapes=[
             pltpu.VMEM((count // KEY_BLOCK, KEY_BLOCK, 2 * LANES), bf16),
@@ -303,8 +326,8 @@
             pltpu.VMEM((count, half), f32),
             pltpu.VMEM((qblocks, 1, LANES), f32),
             pltpu.VMEM((qblocks, 1, LANES), f32),
-            pltpu.SemaphoreType.DMA((devices,)),
-            pltpu.SemaphoreType.DMA((devices,)),
+            pltpu.SemaphoreType.DMA((qblocks, devices)),
+            pltpu.SemaphoreType.DMA((qblocks, devices)),
             pltpu.SemaphoreType.DMA((2,)),
             pltpu.SemaphoreType.DMA((qblocks,)),
             pltpu.SemaphoreType.DMA((qblocks,)),
@@ -314,7 +337,7 @@
             collective_id=0, has_side_effects=True, vmem_limit_bytes=60 * 1024 * 1024
         ),
     )(
-        chosen_owner[0], chosen_part[0], row_data, query_weight, key_weight, value_weight,
+        ids, row_data, query_weight, key_weight, value_weight,
         out_weight, norm_gain[None], cosine, sine,
     )
     return result[None]

time: 47.2 us -> 39.3 us (0.83)
  Pallas kernels: 38.6 us -> 32.6 us
  local copies, waits for them, and re-layouts: 5.38 us -> 3.35 us
    pallas_call x1, Pallas kernels: 38.6 us -> 32.6 us  [body(): pl.pallas_call(functools.partial(kernel, devices), out_shape=jax.ShapeDty...]
    squeeze x2 -> x0, local copies, waits for them, and re-layouts: 2.71 us -> none  [the longest x1 1.36 us: body(): chosen_owner[0]]
    mul x0 -> x1, other arithmetic: none -> 2.49 us  [body(): sine = jnp.where(lane % HEAD_DIM < half_dim, -1.0, 1.0) * jnp.sin(angles)]
    concatenate x1 -> x0, other arithmetic: 1.56 us -> none  [body(): cosine = jnp.concatenate([cosine] * (LANES // half_dim), axis=1)]
    neg x1 -> x0, other arithmetic: 1.44 us -> none  [body(): sine = jnp.concatenate([-sine, sine] * (LANES // HEAD_DIM), axis=1)]
    select_n x0 -> x2, other arithmetic: none -> 0.71 us  [the longest x1 0.71 us: body(): jnp.where(chosen_owner[0] >= 0, chosen_owner[0] * (count // KEY_BLOCK) +...]
    select_n x0 -> x1, local copies, waits for them, and re-layouts: none -> 0.68 us  [body(): jnp.where(chosen_owner[0] >= 0, chosen_owner[0] * (count // KEY_BLOCK) +...]
where the time goes in v2:
time: 39.3 us; the launch traced here: 39.1 us
  Pallas kernels  32.6 us (83%)
  local copies, waits for them, and re-layouts  3.35 us (9%)
  other arithmetic  3.21 us (8%)
    pallas_call x1, Pallas kernels, body(): pl.pallas_call(functools.partial(kernel, devices), out_shape=jax.ShapeDty...  32.6 us
    unnamed x1, local copies, waits for them, and re-layouts  2.67 us
    mul x1, other arithmetic, body(): sine = jnp.where(lane % HEAD_DIM < half_dim, -1.0, 1.0) * jnp.sin(angles)  2.49 us

profile of v2, /device:TPU:27, one launch (start us, length us, event | category | flops | bytes accessed | tf_op | source)
XLA Modules:
  0.0 39.1 jit_solution(6381049856282538029)
XLA Ops:
  0.0 0.7 %select_bitcast_fusion = s32[24,4]{0,1:T(4,128)S(1)} fusion(s32[1,24,4]{1,2,0:T(4,128)} %param.15, s32[1,24,4]{1,2,0:T(4,128)} %param.14), kind=kLoop, calls=%fused_computation.4 | loop fusion | flops 384 | bytes 1152 | tf_op jit(solution)/shard_map/jit(_where)/select_n | solution.py:305
  0.7 0.7 %copy.9.ids_ref = s32[24,4]{1,0:T(8,128)} copy(s32[24,4]{0,1:T(4,128)S(1)} %select_bitcast_fusion) | data formatting | bytes 768 | tf_op jit(solution)/shard_map/jit(_where)/select_n | solution.py:305
  1.4 2.5 %fusion = (f32[768,128]{1,0:T(8,128)}, f32[768,128]{1,0:T(8,128)}) fusion(f32[128]{0:T(128)S(1)} %get-tuple-element.7, f32[128]{0:T(128)S(1)} %get-tuple-element.8, f32[768]{0:T(1024)S(1)} %add_convert_fusion), kind=kLoop, calls=%fused_computation.2 | loop fusion | flops 196608 | bytes 790528 | tf_op jit(solution)/shard_map/mul | solution.py:304
  3.9 32.6 %shard_map.82 = bf16[768,1024]{1,0:T(8,128)(2,1)} custom-call(s32[24,4]{1,0:T(8,128)} %copy.9.ids_ref, bf16[768,2048]{1,0:T(8,128)(2,1)} %bitcast.6, bf16[2048,512]{1,0:T(8,128)(2,1)} %wq.1, bf16[2048,128]{1,0:T(8,128)(2,1)} %wk.1, bf16[2048,128]{1,0:T(8,128)(2,1)} %wv.1, bf16[512,2048]{1,0:T(8,128)(2,1)} %ow.1, f32[1,1024]{1,0:T(1,128)} %bitcast.7, ...), custom_call_target="tpu_custom_call" | custom-call | tf_op jit(solution)/shard_map/pallas_call | solution.py:313
  36.5 2.7 %copy.11 = bf16[1,768,1024]{2,1,0:T(8,128)(2,1)} copy(bf16[1,768,1024]{2,1,0:T(8,128)(2,1)} %bitcast.5) | data formatting | bytes 3145728
  (2 shorter events, 0.0 us)

commit v3 on v2

--- a/solution.py
+++ b/solution.py
@@ -39,7 +39,8 @@
 
 
 def kernel(
-    devices, ids_ref, tok, wq, wk, wv, ow, gain, cosine, sine, out,
+    devices, ids_ref, tok_hbm, wq_hbm, wk_hbm, wv_hbm, ow_hbm, gain, cosine, sine, out,
+    tok, wq, wkv, ow, tok_sems, weight_sems,
     kv, send, pool, queries, mix, mix_other, ow_other, proj, ss, ss_other,
     kv_send, kv_recv, ow_sems, mix_send, mix_recv, ss_sems,
 ):
@@ -54,6 +55,25 @@
     row_steps = tokens // ROWS
     per_q = QUERY_BLOCK // KEY_BLOCK
 
+    key_width = wk_hbm.shape[1]
+
+    def tok_copy(r):
+        rows = pl.ds(pl.multiple_of(r * ROWS, ROWS), ROWS)
+        return pltpu.make_async_copy(tok_hbm.at[rows], tok.at[rows], tok_sems.at[r])
+
+    wk_copy = pltpu.make_async_copy(wk_hbm, wkv.at[:, pl.ds(0, key_width)], weight_sems.at[0])
+    wv_copy = pltpu.make_async_copy(
+        wv_hbm, wkv.at[:, pl.ds(key_width, key_width)], weight_sems.at[1]
+    )
+    wq_copy = pltpu.make_async_copy(wq_hbm, wq, weight_sems.at[2])
+    ow_load = pltpu.make_async_copy(ow_hbm, ow, weight_sems.at[3])
+    wk_copy.start()
+    wv_copy.start()
+    for r in range(row_steps):
+        tok_copy(r).start()
+    wq_copy.start()
+    ow_load.start()
+
     barrier = pltpu.get_barrier_semaphore()
 
     @pl.loop(0, devices)
@@ -64,12 +84,16 @@
 
     pl.semaphore_signal(barrier, inc=1, device_id={"tp": other}, device_id_type=MESH)
 
+    wk_copy.wait()
+    wv_copy.wait()
+
     @pl.loop(0, row_steps)
     def _(r):
+        tok_copy(r).wait()
         rows = pl.ds(pl.multiple_of(r * ROWS, ROWS), ROWS)
         both = jnp.dot(
             tok[rows, :],
-            jnp.concatenate([wk[...], wv[...]], axis=1),
+            wkv[...],
             preferred_element_type=jnp.float32,
         )
         keys = turn(both[:, :LANES], cosine[rows, :], sine[rows, :])
@@ -124,7 +148,9 @@
         device_id={"tp": other},
         device_id_type=MESH,
     )
+    ow_load.wait()
     ow_copy.start()
+    wq_copy.wait()
 
     @pl.loop(0, row_steps)
     def _(r):
@@ -139,7 +165,7 @@
                     part[:, k * LANES : (k + 1) * LANES], cosine[rows, :], sine[rows, :]
                 ).astype(jnp.bfloat16)
 
-    kv_heads = wk.shape[1] // HEAD_DIM
+    kv_heads = key_width // HEAD_DIM
     slices = wq.shape[1] // LANES // kv_heads
     key_count = devices * KEY_BLOCK + QUERY_BLOCK
 
@@ -313,9 +339,15 @@
     result = pl.pallas_call(
         functools.partial(kernel, devices),
         out_shape=jax.ShapeDtypeStruct((count, half), bf16),
-        in_specs=[smem] + [vmem] * 8,
+        in_specs=[smem] + [pl.BlockSpec(memory_space=pl.ANY)] * 5 + [vmem] * 3,
         out_specs=vmem,
         scratch_shapes=[
+            pltpu.VMEM(row_data.shape, bf16),
+            pltpu.VMEM(query_weight.shape, bf16),
+            pltpu.VMEM((key_weight.shape[0], 2 * key_weight.shape[1]), bf16),
+            pltpu.VMEM(out_weight.shape, bf16),
+            pltpu.SemaphoreType.DMA((count // ROWS,)),
+            pltpu.SemaphoreType.DMA((4,)),
             pltpu.VMEM((count // KEY_BLOCK, KEY_BLOCK, 2 * LANES), bf16),
             pltpu.VMEM((devices * qblocks, KEY_BLOCK, 2 * LANES), bf16),
             pltpu.VMEM((devices * qblocks, KEY_BLOCK, 2 * LANES), bf16),

time: 39.3 us -> 37.2 us (0.947)
  Pallas kernels: 32.6 us -> 30.4 us
    pallas_call x1, Pallas kernels: 32.6 us -> 30.4 us  [body(): pl.pallas_call(functools.partial(kernel, devices), out_shape=jax.ShapeDty...]
where the time goes in v3:
time: 37.2 us; the launch traced here: 37 us
  Pallas kernels  30.4 us (82%)
  local copies, waits for them, and re-layouts  3.35 us (9%)
  other arithmetic  3.21 us (9%)
    pallas_call x1, Pallas kernels, body(): pl.pallas_call(functools.partial(kernel, devices), out_shape=jax.ShapeDty...  30.4 us
    unnamed x1, local copies, waits for them, and re-layouts  2.67 us
    mul x1, other arithmetic, body(): sine = jnp.where(lane % HEAD_DIM < half_dim, -1.0, 1.0) * jnp.sin(angles)  2.49 us

profile of v3, /device:TPU:27, one launch (start us, length us, event | category | flops | bytes accessed | tf_op | source)
XLA Modules:
  0.0 37.0 jit_solution(1158586705394147721)
XLA Ops:
  0.0 0.7 %select_bitcast_fusion = s32[24,4]{0,1:T(4,128)S(1)} fusion(s32[1,24,4]{1,2,0:T(4,128)} %param.15, s32[1,24,4]{1,2,0:T(4,128)} %param.14), kind=kLoop, calls=%fused_computation.4 | loop fusion | flops 384 | bytes 1152 | tf_op jit(solution)/shard_map/jit(_where)/select_n | solution.py:331
  0.7 0.7 %copy.9.ids_ref = s32[24,4]{1,0:T(8,128)} copy(s32[24,4]{0,1:T(4,128)S(1)} %select_bitcast_fusion) | data formatting | bytes 768 | tf_op jit(solution)/shard_map/jit(_where)/select_n | solution.py:331
  1.4 2.5 %fusion = (f32[768,128]{1,0:T(8,128)}, f32[768,128]{1,0:T(8,128)}) fusion(f32[128]{0:T(128)S(1)} %get-tuple-element.7, f32[128]{0:T(128)S(1)} %get-tuple-element.8, f32[768]{0:T(1024)S(1)} %add_convert_fusion), kind=kLoop, calls=%fused_computation.2 | loop fusion | flops 196608 | bytes 790528 | tf_op jit(solution)/shard_map/mul | solution.py:330
  3.9 30.4 %shard_map.82 = bf16[768,1024]{1,0:T(8,128)(2,1)} custom-call(s32[24,4]{1,0:T(8,128)} %copy.9.ids_ref, bf16[768,2048]{1,0:T(8,128)(2,1)} %bitcast.6, bf16[2048,512]{1,0:T(8,128)(2,1)} %wq_hbm.1, bf16[2048,128]{1,0:T(8,128)(2,1)} %wk_hbm.1, bf16[2048,128]{1,0:T(8,128)(2,1)} %wv_hbm.1, bf16[512,2048]{1,0:T(8,128)(2,1)} %ow_hbm.1, f32[1,1024]{1,0:T(1,128)} %bitcast.7, ...), custom_call_target="tpu_custom_call" | custom-call | tf_op jit(solution)/shard_map/pallas_call | solution.py:339
  34.3 2.7 %copy.11 = bf16[1,768,1024]{2,1,0:T(8,128)(2,1)} copy(bf16[1,768,1024]{2,1,0:T(8,128)(2,1)} %bitcast.5) | data formatting | bytes 3145728
  (2 shorter events, 0.0 us)

commit v4 on v3

--- a/solution.py
+++ b/solution.py
@@ -2,6 +2,7 @@
 
 import jax
 import jax.numpy as jnp
+import numpy as np
 from jax import lax
 from jax.experimental import pallas as pl
 from jax.experimental.pallas import tpu as pltpu
@@ -39,7 +40,8 @@
 
 
 def kernel(
-    devices, ids_ref, tok_hbm, wq_hbm, wk_hbm, wv_hbm, ow_hbm, gain, cosine, sine, out,
+    devices, ids_ref, tok_hbm, wq_hbm, wk_hbm, wv_hbm, ow_hbm, gain, far_cos, far_sin, near_cos, near_sin, out,
+    cosine, sine,
     tok, wq, wkv, ow, tok_sems, weight_sems,
     kv, send, pool, queries, mix, mix_other, ow_other, proj, ss, ss_other,
     kv_send, kv_recv, ow_sems, mix_send, mix_recv, ss_sems,
@@ -83,6 +85,12 @@
             pl.semaphore_signal(barrier, inc=1, device_id={"kv": j}, device_id_type=MESH)
 
     pl.semaphore_signal(barrier, inc=1, device_id={"tp": other}, device_id_type=MESH)
+
+    @pl.loop(0, qblocks)
+    def _(b):
+        rows = pl.ds(pl.multiple_of(b * QUERY_BLOCK, QUERY_BLOCK), QUERY_BLOCK)
+        cosine[rows, :] = far_cos[b] * near_cos[...] - far_sin[b] * near_sin[...]
+        sine[rows, :] = far_sin[b] * near_cos[...] + far_cos[b] * near_sin[...]
 
     wk_copy.wait()
     wv_copy.wait()
@@ -321,13 +329,16 @@
     count = row_data.shape[0]
     devices = lax.axis_size("kv")
     qblocks = count // QUERY_BLOCK
-    positions = lax.axis_index("kv") * count + jnp.arange(count, dtype=jnp.int32)
     half_dim = HEAD_DIM // 2
-    lane = jnp.arange(LANES, dtype=jnp.int32)
-    frequency = rope_base ** (-(lane % half_dim).astype(jnp.float32) / half_dim)
-    angles = positions.astype(jnp.float32)[:, None] * frequency
-    cosine = jnp.cos(angles)
-    sine = jnp.where(lane % HEAD_DIM < half_dim, -1.0, 1.0) * jnp.sin(angles)
+    lane = np.arange(LANES)
+    frequency = (rope_base ** (-(lane % half_dim) / half_dim)).astype(np.float32)
+    sign = np.where(lane % HEAD_DIM < half_dim, -1.0, 1.0).astype(np.float32)
+    inner = np.arange(QUERY_BLOCK)[:, None] * frequency.astype(np.float64)
+    near_cos = np.cos(inner).astype(np.float32)
+    near_sin = (sign * np.sin(inner)).astype(np.float32)
+    starts = lax.axis_index("kv") * count + QUERY_BLOCK * jnp.arange(qblocks, dtype=jnp.int32)
+    angles = starts.astype(jnp.float32)[:, None, None] * frequency
+    far_cos, far_sin = jnp.cos(angles), sign * jnp.sin(angles)
     ids = jnp.where(
         chosen_owner[0] >= 0, chosen_owner[0] * (count // KEY_BLOCK) + chosen_part[0], -1
     )
@@ -339,9 +350,11 @@
     result = pl.pallas_call(
         functools.partial(kernel, devices),
         out_shape=jax.ShapeDtypeStruct((count, half), bf16),
-        in_specs=[smem] + [pl.BlockSpec(memory_space=pl.ANY)] * 5 + [vmem] * 3,
+        in_specs=[smem] + [pl.BlockSpec(memory_space=pl.ANY)] * 5 + [vmem] * 5,
         out_specs=vmem,
         scratch_shapes=[
+            pltpu.VMEM((count, LANES), f32),
+            pltpu.VMEM((count, LANES), f32),
             pltpu.VMEM(row_data.shape, bf16),
             pltpu.VMEM(query_weight.shape, bf16),
             pltpu.VMEM((key_weight.shape[0], 2 * key_weight.shape[1]), bf16),
@@ -370,7 +383,8 @@
         ),
     )(
         ids, row_data, query_weight, key_weight, value_weight,
-        out_weight, norm_gain[None], cosine, sine,
+        out_weight, norm_gain[None], far_cos, far_sin,
+        jnp.asarray(near_cos), jnp.asarray(near_sin),
     )
     return result[None]
 

time: 37.2 us -> 36 us (0.968)
  other arithmetic: 3.21 us -> 2.14 us
    mul x1, other arithmetic: 2.49 us -> 1.43 us  [body(): far_cos, far_sin = (jnp.cos(angles), sign * jnp.sin(angles))]
where the time goes in v4:
time: 36 us; the launch traced here: 35.8 us
  Pallas kernels  30.3 us (84%)
  local copies, waits for them, and re-layouts  3.35 us (9%)
  other arithmetic  2.14 us (6%)
    pallas_call x1, Pallas kernels, body(): pl.pallas_call(functools.partial(kernel, devices), out_shape=jax.ShapeDty...  30.3 us
    unnamed x1, local copies, waits for them, and re-layouts  2.67 us
    mul x1, other arithmetic, body(): far_cos, far_sin = (jnp.cos(angles), sign * jnp.sin(angles))  1.43 us

profile of v4, /device:TPU:27, one launch (start us, length us, event | category | flops | bytes accessed | tf_op | source)
XLA Modules:
  0.0 35.8 jit_solution(9237270610033573965)
XLA Ops:
  0.0 0.7 %select_bitcast_fusion = s32[24,4]{0,1:T(4,128)S(1)} fusion(s32[1,24,4]{1,2,0:T(4,128)} %param.19, s32[1,24,4]{1,2,0:T(4,128)} %param.18), kind=kLoop, calls=%fused_computation.3 | loop fusion | flops 384 | bytes 1152 | tf_op jit(solution)/shard_map/jit(_where)/select_n | solution.py:342
  0.7 1.4 %fusion = (f32[6,1,128]{2,1,0:T(1,128)}, f32[6,1,128]{2,1,0:T(1,128)}) fusion(f32[128]{0:T(128)} %constant.25.clone, f32[128]{0:T(128)} %constant.24.clone, f32[6]{0:T(128)S(1)} %add_convert_fusion), kind=kLoop, calls=%fused_computation.2 | loop fusion | flops 1536 | bytes 7192 | tf_op jit(solution)/shard_map/mul | solution.py:341
  2.1 0.7 %copy.13.ids_ref = s32[24,4]{1,0:T(8,128)} copy(s32[24,4]{0,1:T(4,128)S(1)} %select_bitcast_fusion) | data formatting | bytes 768 | tf_op jit(solution)/shard_map/jit(_where)/select_n | solution.py:342
  2.8 30.3 %shard_map.118 = bf16[768,1024]{1,0:T(8,128)(2,1)} custom-call(s32[24,4]{1,0:T(8,128)} %copy.13.ids_ref, bf16[768,2048]{1,0:T(8,128)(2,1)} %bitcast.6, bf16[2048,512]{1,0:T(8,128)(2,1)} %wq_hbm.1, bf16[2048,128]{1,0:T(8,128)(2,1)} %wk_hbm.1, bf16[2048,128]{1,0:T(8,128)(2,1)} %wv_hbm.1, bf16[512,2048]{1,0:T(8,128)(2,1)} %ow_hbm.1, f32[1,1024]{1,0:T(1,128)} %bitcast.7, ...), custom_call_target="tpu_custom_call" | custom-call | tf_op jit(solution)/shard_map/pallas_call | solution.py:350
  33.1 2.7 %copy.15 = bf16[1,768,1024]{2,1,0:T(8,128)(2,1)} copy(bf16[1,768,1024]{2,1,0:T(8,128)(2,1)} %bitcast.5) | data formatting | bytes 3145728
  (1 shorter events, 0.0 us)
